TPU v7x, 32 devices: a whole 2x2x4 slice. The times are simulated.
32 devices in a mesh: kv: 16 (over z, y, x), tp: 2 (over core).
Axes of the slice: x: 2, y: 2, z: 4, core: 2. Of those that a mesh axis runs over, the one named last changes fastest.
Arguments:
- tokens: bfloat16 [16, 4096], P(None, ('kv', 'tp')), may hold values from -12 to 12
- lengths: int32 [16], replicated, may hold values from 1 to 2048, 10922 in all
- attn_gain: bfloat16 [4096], P('kv'), may hold values from 0.099609375 to 1.8984375
- w_query: bfloat16 [4096, 2048], P('kv', 'tp'), may hold values from -0.09375 to 0.09375
- w_key: bfloat16 [4096, 2048], P('kv', 'tp'), may hold values from -0.09375 to 0.09375
- w_value: bfloat16 [4096, 4096], P('kv', 'tp'), may hold values from -0.09375 to 0.09375
- w_gate: bfloat16 [4096, 4096], P('kv', 'tp'), may hold values from -0.09375 to 0.09375
- decay_rate: float32 [32], P('tp'), may hold values from 4.8828125e-05 to 0.05
- key_cache: bfloat16 [16, 2048, 2048], P(None, 'kv', 'tp'), may hold values from -6 to 6
- value_cache: bfloat16 [16, 2048, 4096], P(None, 'kv', 'tp'), may hold values from -6 to 6
- head_gain: bfloat16 [4096], P('tp'), may hold values from 0.099609375 to 1.8984375
- w_output: bfloat16 [4096, 4096], P('tp', 'kv'), may hold values from -0.09375 to 0.09375
- mlp_gain: bfloat16 [4096], replicated, may hold values from 0.099609375 to 1.8984375
- w_up: bfloat16 [4096, 16384], P(None, ('kv', 'tp')), may hold values from -0.09375 to 0.09375
- w_down: bfloat16 [16384, 4096], P(('kv', 'tp')), may hold values from -0.09375 to 0.09375
Outputs:
- layer_out: bfloat16 [16, 4096], P(None, ('kv', 'tp'))
Inputs may be any that keep to these rules, and one draw needn't show every extreme that they name: Sequence s has lengths[s] live cache positions, 0 to lengths[s] - 1, and its new token stands at position lengths[s]; the longest fills all 2048 positions.
All inputs are finite; a program needn't handle non-finite values.
Results may differ from a plain program's by a relative error of at most 0.012.
Values may be sent and summed in bfloat16 or wider, within the bound.
A program may use at most 64 MiB of HBM per device.

v0:
```python
import jax
import jax.numpy as jnp
from jax import lax
from jax.sharding import PartitionSpec as P

WIDTH = 4096
HEAD_KEY = 64
HEAD_VALUE = 128
EPS = 1e-05
THETA = 10000.0


def rotate(flattened, position):
    row_count = flattened.shape[0]
    grouped = flattened.reshape(row_count, -1, HEAD_KEY)
    halfway = HEAD_KEY // 2
    inverse = jnp.power(THETA, -jnp.arange(halfway, dtype=jnp.float32) / halfway)
    angles = position.astype(jnp.float32)[:, None] * inverse[None, :]
    cosine = jnp.cos(angles)[:, None, :]
    sine_part = jnp.sin(angles)[:, None, :]
    first_half = grouped[..., :halfway]
    second_half = grouped[..., halfway:]
    turned = jnp.concatenate(
        [
            first_half * cosine - second_half * sine_part,
            second_half * cosine + first_half * sine_part,
        ],
        -1,
    )
    return turned.reshape(row_count, -1)


def affine(product_sum, column, average, inverse_std):
    return inverse_std[:, None] * (product_sum - average[:, None] * column[None, :])


def on_device(
    tokens,
    lengths,
    attn_gain,
    w_query,
    w_key,
    w_value,
    w_gate,
    decay_rate,
    key_cache,
    value_cache,
    head_gain,
    w_output,
    mlp_gain,
    w_up,
    w_down,
):
    seq_count = tokens.shape[0]
    head_count = decay_rate.shape[0]
    span_rows = key_cache.shape[1]
    block_cols = lax.all_gather(tokens, "tp", axis=1, tiled=True)
    widened = block_cols.astype(jnp.float32)
    scaled = (widened * attn_gain.astype(jnp.float32)).astype(jnp.bfloat16)
    gain_row = attn_gain[None, :]
    part_query = jnp.dot(scaled, w_query, preferred_element_type=jnp.float32)
    part_key = jnp.dot(scaled, w_key, preferred_element_type=jnp.float32)
    part_value = jnp.dot(scaled, w_value, preferred_element_type=jnp.float32)
    part_gate = jnp.dot(scaled, w_gate, preferred_element_type=jnp.float32)
    col_query = jnp.dot(gain_row, w_query, preferred_element_type=jnp.float32)[0]
    col_key = jnp.dot(gain_row, w_key, preferred_element_type=jnp.float32)[0]
    col_value = jnp.dot(gain_row, w_value, preferred_element_type=jnp.float32)[0]
    col_gate = jnp.dot(gain_row, w_gate, preferred_element_type=jnp.float32)[0]
    (
        sum_query,
        sum_key,
        sum_value,
        sum_gate,
        csum_query,
        csum_key,
        csum_value,
        csum_gate,
        first_moment,
        second_moment,
    ) = lax.psum(
        (
            part_query,
            part_key,
            part_value,
            part_gate,
            col_query,
            col_key,
            col_value,
            col_gate,
            jnp.sum(widened, -1),
            jnp.sum(widened * widened, -1),
        ),
        "kv",
    )
    average = first_moment / WIDTH
    inverse_std = lax.rsqrt(second_moment / WIDTH - average * average + EPS)
    query_rows = rotate(affine(sum_query, csum_query, average, inverse_std), lengths).astype(
        jnp.bfloat16
    )
    new_key = rotate(affine(sum_key, csum_key, average, inverse_std), lengths).astype(jnp.bfloat16)
    new_value = affine(sum_value, csum_value, average, inverse_std).astype(jnp.bfloat16)
    gate_value = affine(sum_gate, csum_gate, average, inverse_std)
    queries = query_rows.reshape(seq_count, head_count, HEAD_KEY)
    keys_local = key_cache.reshape(seq_count, span_rows, head_count, HEAD_KEY)
    values_local = value_cache.reshape(seq_count, span_rows, head_count, HEAD_VALUE)
    scores = jnp.einsum(
        "bhd,bjhd->bhj", queries, keys_local, preferred_element_type=jnp.float32
    ) * HEAD_KEY ** (-0.5)
    places = lax.axis_index("kv") * span_rows + jnp.arange(span_rows, dtype=jnp.int32)
    distance = jnp.maximum(lengths[:, None] - places[None, :], 0).astype(jnp.float32)
    live_mask = (places[None, :] < lengths[:, None])[:, None, :]
    weights = jnp.where(live_mask, jnp.exp(-decay_rate[None, :, None] * distance[:, None, :]), 0.0)
    coefficients = (scores * weights).astype(jnp.bfloat16)
    partial_out = jnp.einsum(
        "bhj,bjhe->bhe", coefficients, values_local, preferred_element_type=jnp.float32
    )
    cached = lax.psum(partial_out, "kv")
    own_score = jnp.sum(
        queries.astype(jnp.float32)
        * new_key.reshape(seq_count, head_count, HEAD_KEY).astype(jnp.float32),
        -1,
    ) * HEAD_KEY ** (-0.5)
    retained = cached + own_score[:, :, None] * new_value.reshape(
        seq_count, head_count, HEAD_VALUE
    ).astype(jnp.float32)
    centered = retained - jnp.mean(retained, -1, keepdims=True)
    normed = (
        centered
        * lax.rsqrt(jnp.mean(centered * centered, -1, keepdims=True) + EPS)
        * head_gain.reshape(head_count, HEAD_VALUE).astype(jnp.float32)
    )
    gated_out = (jax.nn.silu(gate_value) * normed.reshape(seq_count, -1)).astype(jnp.bfloat16)
    partial_branch = jnp.dot(gated_out, w_output, preferred_element_type=jnp.float32)
    branch = lax.psum_scatter(
        partial_branch.astype(jnp.bfloat16), "tp", scatter_dimension=1, tiled=True
    ).astype(jnp.float32)
    own_residual = (tokens.astype(jnp.float32) + branch).astype(jnp.bfloat16)
    piece_wide = lax.all_gather(own_residual, ("kv", "tp"), axis=1, tiled=True).astype(jnp.float32)
    scaled_piece = (piece_wide * mlp_gain.astype(jnp.float32)).astype(jnp.bfloat16)
    totals = (
        jnp.dot(scaled_piece, w_up, preferred_element_type=jnp.float32),
        jnp.sum(piece_wide, -1),
        jnp.sum(piece_wide * piece_wide, -1),
    )
    accumulated, first_sum, second_sum = totals
    mid_average = first_sum / WIDTH
    mid_inverse = lax.rsqrt(second_sum / WIDTH - mid_average * mid_average + EPS)
    column_up = jnp.dot(mlp_gain[None, :], w_up, preferred_element_type=jnp.float32)[0]
    hidden = jnp.square(
        jax.nn.relu(affine(accumulated, column_up, mid_average, mid_inverse))
    ).astype(jnp.bfloat16)
    down_terms = jnp.dot(hidden, w_down, preferred_element_type=jnp.float32)
    kv_block = lax.psum_scatter(down_terms, "kv", scatter_dimension=1, tiled=True)
    mixer_sum = lax.psum_scatter(kv_block, "tp", scatter_dimension=1, tiled=True)
    return (own_residual.astype(jnp.float32) + mixer_sum).astype(jnp.bfloat16)


def solution(mesh):
    in_specs = (
        P(None, ("kv", "tp")),
        P(),
        P("kv"),
        P("kv", "tp"),
        P("kv", "tp"),
        P("kv", "tp"),
        P("kv", "tp"),
        P("tp"),
        P(None, "kv", "tp"),
        P(None, "kv", "tp"),
        P("tp"),
        P("tp", "kv"),
        P(),
        P(None, ("kv", "tp")),
        P(("kv", "tp"), None),
    )
    out_specs = P(None, ("kv", "tp"))
    return jax.shard_map(
        on_device, mesh=mesh, in_specs=in_specs, out_specs=out_specs, check_vma=False
    )
```

profile of v0, /device:TPU:0, one launch (start us, length us, event | category | flops | bytes accessed | tf_op | source)
XLA Modules:
  0.0 387.7 jit_solution(13604022745507007239)
XLA Ops:
  6.5 2.3 all_gather.6
  9.5 1.8 fusion.36
  14.4 1.2 fusion.44
  15.8 0.9 fusion.32
  16.7 1.5 fusion.43
  18.2 0.9 fusion.38
  20.2 78.5 %all-reduce = (f32[1024]{0:T(1024)S(1)}, f32[16]{0:T(128)S(1)}, f32[16]{0:T(128)S(1)}, f32[2048]{0:T(1024)S(1)}, f32[1024]{0:T(1024)S(1)}, /*index=5*/f32[2048]{0:T(1024)S(1)}) all-reduce(f32[1024]{0:T(1024)S(1)} %bitcast.62, f32[16]{0:T(128)S(1)} %get-tuple-element.8, ...), channel_id=1, replica_groups=mesh['kv'=16,'tp'=2] {'kv'}, use_global_device_ids=true, to_apply=%region_7.0 | all-reduce | flops 6176 | bytes 49408 | tf_op jit(solution)/shard_map/psum | solution.py:80
  98.7 6.4 %copy.17 = bf16[16,128,1024]{1,2,0:T(8,128)(2,1)} copy(bf16[16,128,1024]{2,1,0:T(8,128)(2,1)} %param.23) | data formatting | bytes 8388608 | tf_op args[8]
  105.1 13.9 %all-reduce.5.cloned.1.call-done = f32[16,1024]{1,0:T(8,128)} async-done(((f32[16,1024]{1,0:T(8,128)}), f32[16,1024]{1,0:T(8,128)}) %all-reduce.5.cloned.1.call-update) | async-done | bytes 65552 | tf_op jit(solution)/shard_map/psum | solution.py:80
  119.1 0.9 subtract_multiply_fusion.1
  120.3 3.4 fusion.14
  123.8 6.4 %fusion = f32[16,16,1,128]{3,2,1,0:T(1,128)} fusion(bf16[16,16,128,1]{2,1,0,3:T(8,128)(2,1)S(1)} %fusion.18, bf16[16,128,2048]{2,1,0:T(8,128)(2,1)} %param.24), kind=kOutput, calls=%fused_computation | convolution fusion | flops 8388608 | bytes 8585216 | tf_op jit(solution)/shard_map/bhj,bjhe->bhe/dot_general | solution.py:114
  130.3 109.1 %all-reduce.7.cloned.1.call-done = (f32[16,16,128]{2,1,0:T(8,128)}, f32[16,2048]{1,0:T(8,128)}, f32[16,1024]{1,0:T(8,128)}, f32[16,2048]{1,0:T(8,128)}) async-done(((f32[16,16,128]{2,1,0:T(8,128)}, f32[16,2048]{1,0:T(8,128)}, f32[16,1024]{1,0:T(8,128)}, f32[16,2048]{1,0:T(8,128)}), (f32[16,16,128]{2,1,0:T(8,128)}, f32[16,2048]{1,0:T(8,128)}, f32[16,1024]{1,0:T(8,128)}, ...) | async-done | bytes 458768 | tf_op jit(solution)/shard_map/psum | solution.py:117
  239.5 0.9 subtract_multiply_fusion
  240.8 1.0 convert_bitcast_fusion
  241.9 1.0 fusion.42
  243.3 1.2 convolution_convert_fusion
  245.4 2.8 fusion.47
  248.2 3.9 %reduce-scatter.10.cloned.1.call-done = bf16[128,16]{1,0:T(8,128)(2,1)} async-done(((bf16[256,16]{1,0:T(8,128)(2,1)}), bf16[128,16]{1,0:T(8,128)(2,1)}) %reduce-scatter.10.cloned.1.call-update) | async-done | bytes 4112
  253.0 42.0 %all_gather.7 = bf16[16,4096]{1,0:T(8,128)(2,1)S(1)} all-gather(bf16[16,128]{1,0:T(8,128)(2,1)S(1)} %add_convert_fusion.3), channel_id=1, replica_groups=mesh['kv'=16,'tp'=2] {'kv','tp'}, dimensions={1}, use_global_device_ids=true | all-gather | bytes 135168 | tf_op jit(solution)/shard_map/all_gather | solution.py:138
  295.1 5.5 %fusion.7 = f32[16,4096]{1,0:T(8,128)} fusion(bf16[512,4096]{1,0:T(8,128)(2,1)} %param.29, bf16[4096,512]{1,0:T(8,128)(2,1)} %param.28, bf16[16,4096]{1,0:T(8,128)(2,1)S(1)} %all_gather.7, f32[4096]{0:T(1024)S(1)} %convert_element_type.105, f32[512]{0:T(512)S(1)} %bitcast.64, f32[16]{0:T(128)S(1)} %get-tuple-element.28, f32[16]{0:T(128)S(1)} %get-tuple-element.27), kind=kOutput, calls=%fused_computation.8 | convolution fusion | flops 134463488 | bytes 8800384 | tf_op jit(solution)/shard_map/dot_general | solution.py:152
  300.7 73.3 %reduce-scatter.6.cloned.1.call-done = f32[16,256]{1,0:T(8,128)} async-done(((f32[16,4096]{1,0:T(8,128)}), f32[16,256]{1,0:T(8,128)}) %reduce-scatter.6.cloned.1.call-update) | async-done | bytes 16400 | tf_op jit(solution)/shard_map/reduce_scatter | solution.py:153
  374.0 5.9 %reduce-scatter.8.cloned.1.call-done = f32[16,128]{1,0:T(8,128)} async-done(((f32[16,256]{1,0:T(8,128)}), f32[16,128]{1,0:T(8,128)}) %reduce-scatter.8.cloned.1.call-update) | async-done | bytes 8208 | tf_op jit(solution)/shard_map/reduce_scatter | solution.py:154
  379.9 1.3 add_convert_fusion.2
  (62 shorter events, 8.2 us)
Async XLA Ops:
  6.5 9.1 %copy-start = (bf16[256,2048]{1,0:T(8,128)(2,1)S(1)}, bf16[256,2048]{1,0:T(8,128)(2,1)}, u32[]{:S(2)}) copy-start(bf16[256,2048]{1,0:T(8,128)(2,1)} %param.20) | copy-start | bytes 3145732
  6.5 11.7 %copy-start.1 = (bf16[256,2048]{1,0:T(8,128)(2,1)S(1)}, bf16[256,2048]{1,0:T(8,128)(2,1)}, u32[]{:S(2)}) copy-start(bf16[256,2048]{1,0:T(8,128)(2,1)} %param.21) | copy-start | bytes 3145732
  6.5 12.6 %copy-start.2 = (bf16[256,1024]{1,0:T(8,128)(2,1)S(1)}, bf16[256,1024]{1,0:T(8,128)(2,1)}, u32[]{:S(2)}) copy-start(bf16[256,1024]{1,0:T(8,128)(2,1)} %param.19) | copy-start | bytes 1572868
  6.5 112.5 %all-reduce.5.cloned.1.call-start = ((), (), s32[]{:S(2)}) async-start(), calls=%async_computation.3 | async-start | bytes 131072 | tf_op jit(solution)/shard_map/psum | solution.py:80
  11.4 228.1 %all-reduce.7.cloned.1.call-start = ((), (), s32[]{:S(2)}) async-start(), calls=%async_computation.7 | async-start | bytes 917504 | tf_op jit(solution)/shard_map/psum | solution.py:117
  98.7 6.4 %copy-start.7 = (f32[16]{0:T(128)S(1)}, f32[16]{0:T(128)}, u32[]{:S(2)}) copy-start(f32[16]{0:T(128)} %param.22) | copy-start | bytes 196
  123.8 6.5 %copy-start.4 = (bf16[4096]{0:T(1024)(128)(2,1)S(1)}, bf16[4096]{0:T(1024)(128)(2,1)}, u32[]{:S(2)}) copy-start(bf16[4096]{0:T(1024)(128)(2,1)} %param.27) | copy-start | bytes 24580
  123.8 6.5 %copy-start.6 = (bf16[2048]{0:T(1024)(128)(2,1)S(1)}, bf16[2048]{0:T(1024)(128)(2,1)}, u32[]{:S(2)}) copy-start(bf16[2048]{0:T(1024)(128)(2,1)} %param.25) | copy-start | bytes 12292
  123.8 119.5 %copy-start.3 = (bf16[2048,256]{1,0:T(8,128)(2,1)S(1)}, bf16[2048,256]{1,0:T(8,128)(2,1)}, u32[]{:S(2)}) copy-start(bf16[2048,256]{1,0:T(8,128)(2,1)} %param.26) | copy-start | bytes 3145732
  130.2 121.9 %reduce-scatter.10.cloned.1.call-start = ((), (), s32[]{:S(2)}) async-start(), calls=%async_computation.6 | async-start | bytes 98304
  240.4 12.6 %copy-start.5 = (bf16[16,128]{1,0:T(8,128)(2,1)S(1)}, bf16[16,128]{1,0:T(8,128)(2,1)}, u32[]{:S(2)}) copy-start(bf16[16,128]{1,0:T(8,128)(2,1)} %param.15) | copy-start | bytes 12292
  245.3 128.7 %reduce-scatter.6.cloned.1.call-start = ((), (), s32[]{:S(2)}) async-start(), calls=%async_computation.4 | async-start | bytes 278528 | tf_op jit(solution)/shard_map/reduce_scatter | solution.py:153
  300.6 79.3 %reduce-scatter.8.cloned.1.call-start = ((), (), s32[]{:S(2)}) async-start(), calls=%async_computation.5 | async-start | bytes 24576 | tf_op jit(solution)/shard_map/reduce_scatter | solution.py:154
Sparse Core Ops, SparseCore 0:
  12.8 106.1 all-reduce.4
  130.4 109.0 all-reduce.6
  245.4 6.6 reduce-scatter.9
  300.7 73.1 reduce-scatter.5
  376.0 3.8 reduce-scatter.7
where the time goes:
time: 388 us
  waiting for transfers between devices  206 us (53%)
  blocking collectives  123 us (32%)
  matrix products  26.8 us (7%)
  between operations  13.3 us (3%)
  other arithmetic  9.4 us (2%)
  local copies, waits for them, and re-layouts  8.86 us (2%)
    psum x1, waiting for transfers between devices, on_device(): cached = lax.psum(partial_out, 'kv')  109 us
    psum x1, blocking collectives, on_device(): lax.psum((part_query, part_key, part_value, part_gate, col_query, col_key...  78.5 us
    reduce_scatter x1, waiting for transfers between devices, on_device(): lax.psum_scatter(down_terms, 'kv', scatter_dimension=1, tiled=True)  73.3 us
    all_gather x1, blocking collectives, on_device(): lax.all_gather(own_residual, ('kv', 'tp'), axis=1, tiled=True)  42 us
    psum x1, waiting for transfers between devices, on_device(): lax.psum((part_query, part_key, part_value, part_gate, col_query, col_key...  13.9 us
    unnamed x22, local copies, waits for them, and re-layouts  8.69 us
  transfers between devices with their start and end apart: 5, of which 5 were waited for; matrix products, arithmetic and copies ran while one was open for 5% of the time, Pallas kernels for 0%

commit v1 on v0

--- a/solution.py
+++ b/solution.py
@@ -114,7 +114,7 @@
     partial_out = jnp.einsum(
         "bhj,bjhe->bhe", coefficients, values_local, preferred_element_type=jnp.float32
     )
-    cached = lax.psum(partial_out, "kv")
+    cached = jnp.sum(lax.all_gather(partial_out, "kv"), axis=0)
     own_score = jnp.sum(
         queries.astype(jnp.float32)
         * new_key.reshape(seq_count, head_count, HEAD_KEY).astype(jnp.float32),

time: 388 us -> 346 us (0.89)
  waiting for transfers between devices: 206 us -> 168 us
    psum x1 -> x0, waiting for transfers between devices: 109 us -> none  [on_device(): cached = lax.psum(partial_out, 'kv')]
    all_gather x0 -> x1, waiting for transfers between devices: none -> 59.1 us  [on_device(): cached = jnp.sum(lax.all_gather(partial_out, 'kv'), axis=0)]
    psum x1, waiting for transfers between devices: 13.9 us -> 25.6 us  [on_device(): lax.psum((part_query, part_key, part_value, part_gate, col_query, col_key...]
    unnamed x22 -> x30, local copies, waits for them, and re-layouts: 8.69 us -> 8.7 us
  transfers between devices with their start and end apart: 5 -> 5, of which waited for: 5 -> 5; matrix products, arithmetic and copies ran while one was open for 5% -> 3% of each run, Pallas kernels for 0% -> 0%
where the time goes in v1:
time: 346 us; the launch traced here: 345 us
  waiting for transfers between devices  168 us (49%)
  blocking collectives  123 us (36%)
  matrix products  26 us (8%)
  between operations  13.4 us (4%)
  local copies, waits for them, and re-layouts  9.14 us (3%)
  other arithmetic  6.28 us (2%)
    psum x1, blocking collectives, on_device(): lax.psum((part_query, part_key, part_value, part_gate, col_query, col_key...  78.4 us
    reduce_scatter x1, waiting for transfers between devices, on_device(): lax.psum_scatter(down_terms, 'kv', scatter_dimension=1, tiled=True)  73.3 us
    all_gather x1, waiting for transfers between devices, on_device(): cached = jnp.sum(lax.all_gather(partial_out, 'kv'), axis=0)  59.1 us
    all_gather x1, blocking collectives, on_device(): lax.all_gather(own_residual, ('kv', 'tp'), axis=1, tiled=True)  42 us
    psum x1, waiting for transfers between devices, on_device(): lax.psum((part_query, part_key, part_value, part_gate, col_query, col_key...  25.6 us
    unnamed x30, local copies, waits for them, and re-layouts  8.7 us
  transfers between devices with their start and end apart: 5, of which 5 were waited for; matrix products, arithmetic and copies ran while one was open for 3% of the time, Pallas kernels for 0%

profile of v1, /device:TPU:0, one launch (start us, length us, event | category | flops | bytes accessed | tf_op | source)
XLA Modules:
  0.0 345.4 jit_solution(12407448499209255228)
XLA Ops:
  6.6 2.3 all_gather.12
  8.9 0.7 convert_element_type.87
  9.6 2.1 fusion.38
  11.7 0.9 fusion.44
  12.6 1.8 fusion.40
  14.5 1.8 fusion.42
  16.5 0.7 reshape.195
  18.2 6.4 %copy.17 = bf16[16,128,1024]{1,2,0:T(8,128)(2,1)} copy(bf16[16,128,1024]{2,1,0:T(8,128)(2,1)} %param.23) | data formatting | bytes 8388608 | tf_op args[8]
  24.6 78.4 %all-reduce = (f32[1024]{0:T(1024)S(1)}, f32[16]{0:T(128)S(1)}, f32[16]{0:T(128)S(1)}, f32[2048]{0:T(1024)S(1)}, f32[1024]{0:T(1024)S(1)}, /*index=5*/f32[2048]{0:T(1024)S(1)}) all-reduce(f32[1024]{0:T(1024)S(1)} %bitcast.74, f32[16]{0:T(128)S(1)} %get-tuple-element.8, ...), channel_id=1, replica_groups=mesh['kv'=16,'tp'=2] {'kv'}, use_global_device_ids=true, to_apply=%region_7.0 | all-reduce | flops 6176 | bytes 49408 | tf_op jit(solution)/shard_map/psum | solution.py:80
  103.2 25.6 %all-reduce.4.cloned.1.call-done = (f32[16,1024]{1,0:T(8,128)}, f32[16,2048]{1,0:T(8,128)}, f32[16,1024]{1,0:T(8,128)}, f32[16,2048]{1,0:T(8,128)}) async-done(((f32[16,1024]{1,0:T(8,128)}, f32[16,2048]{1,0:T(8,128)}, f32[16,1024]{1,0:T(8,128)}, f32[16,2048]{1,0:T(8,128)}), (f32[16,1024]{1,0:T(8,128)}, f32[16,2048]{1,0:T(8,128)}, f32[16,1024]{1,0:T(8,128)}, ...) | async-done | bytes 393232 | tf_op jit(solution)/shard_map/psum | solution.py:80
  128.8 1.0 subtract_multiply_fusion
  130.2 3.4 fusion.19
  133.7 6.4 %fusion = f32[16,16,1,128]{3,2,1,0:T(1,128)} fusion(bf16[16,16,128,1]{2,1,0,3:T(8,128)(2,1)S(1)} %fusion.23, bf16[16,128,2048]{2,1,0:T(8,128)(2,1)} %param.24), kind=kOutput, calls=%fused_computation | convolution fusion | flops 8388608 | bytes 8585216 | tf_op jit(solution)/shard_map/bhj,bjhe->bhe/dot_general | solution.py:114
  140.6 59.1 %all-gather.3.cloned.1.call-done = f32[256,16,128]{2,1,0:T(8,128)} async-done(((f32[16,16,128]{2,1,0:T(8,128)}), f32[256,16,128]{2,1,0:T(8,128)}) %all-gather.3.cloned.1.call-update) | async-done | bytes 2097168 | tf_op jit(solution)/shard_map/all_gather | solution.py:117
  199.7 1.7 reduce_sum.76
  202.6 0.7 copy.23
  203.4 2.8 fusion.53
  206.2 3.6 %reduce-scatter.10.cloned.1.call-done = bf16[128,16]{1,0:T(8,128)(2,1)} async-done(((bf16[256,16]{1,0:T(8,128)(2,1)}), bf16[128,16]{1,0:T(8,128)(2,1)}) %reduce-scatter.10.cloned.1.call-update) | async-done | bytes 4112
  209.8 0.8 copy.24
  210.7 42.0 %all_gather.15 = bf16[16,4096]{1,0:T(8,128)(2,1)S(1)} all-gather(bf16[16,128]{1,0:T(8,128)(2,1)S(1)} %add_convert_fusion.3), channel_id=1, replica_groups=mesh['kv'=16,'tp'=2] {'kv','tp'}, dimensions={1}, use_global_device_ids=true | all-gather | bytes 135168 | tf_op jit(solution)/shard_map/all_gather | solution.py:138
  252.8 5.5 %fusion.7 = f32[16,4096]{1,0:T(8,128)} fusion(bf16[512,4096]{1,0:T(8,128)(2,1)} %param.29, bf16[4096,512]{1,0:T(8,128)(2,1)} %param.28, bf16[16,4096]{1,0:T(8,128)(2,1)S(1)} %all_gather.15, f32[4096]{0:T(1024)S(1)} %convert_element_type.105, f32[512]{0:T(512)S(1)} %bitcast.76, f32[16]{0:T(128)S(1)} %get-tuple-element.32, f32[16]{0:T(128)S(1)} %get-tuple-element.31), kind=kOutput, calls=%fused_computation.8 | convolution fusion | flops 134463488 | bytes 8800384 | tf_op jit(solution)/shard_map/dot_general | solution.py:152
  258.4 73.3 %reduce-scatter.6.cloned.1.call-done = f32[16,256]{1,0:T(8,128)} async-done(((f32[16,4096]{1,0:T(8,128)}), f32[16,256]{1,0:T(8,128)}) %reduce-scatter.6.cloned.1.call-update) | async-done | bytes 16400 | tf_op jit(solution)/shard_map/reduce_scatter | solution.py:153
  331.7 5.9 %reduce-scatter.8.cloned.1.call-done = f32[16,128]{1,0:T(8,128)} async-done(((f32[16,256]{1,0:T(8,128)}), f32[16,128]{1,0:T(8,128)}) %reduce-scatter.8.cloned.1.call-update) | async-done | bytes 8208 | tf_op jit(solution)/shard_map/reduce_scatter | solution.py:154
  337.6 1.3 add_convert_fusion.2
  (71 shorter events, 3.8 us)
Async XLA Ops:
  6.5 5.2 %copy-start = (bf16[256,2048]{1,0:T(8,128)(2,1)S(1)}, bf16[256,2048]{1,0:T(8,128)(2,1)}, u32[]{:S(2)}) copy-start(bf16[256,2048]{1,0:T(8,128)(2,1)} %param.21) | copy-start | bytes 3145732
  6.5 10.9 %copy-start.1 = (bf16[256,2048]{1,0:T(8,128)(2,1)S(1)}, bf16[256,2048]{1,0:T(8,128)(2,1)}, u32[]{:S(2)}) copy-start(bf16[256,2048]{1,0:T(8,128)(2,1)} %param.20) | copy-start | bytes 3145732
  6.5 11.3 %copy-start.3 = (bf16[256,1024]{1,0:T(8,128)(2,1)S(1)}, bf16[256,1024]{1,0:T(8,128)(2,1)}, u32[]{:S(2)}) copy-start(bf16[256,1024]{1,0:T(8,128)(2,1)} %param.19) | copy-start | bytes 1572868
  6.5 11.1 %copy-start.2 = (bf16[256,1024]{1,0:T(8,128)(2,1)S(1)}, bf16[256,1024]{1,0:T(8,128)(2,1)}, u32[]{:S(2)}) copy-start(bf16[256,1024]{1,0:T(8,128)(2,1)} %param.18) | copy-start | bytes 1572868
  6.5 11.5 %copy-start.10 = (s32[16]{0:T(128)S(1)}, s32[16]{0:T(128)}, u32[]{:S(2)}) copy-start(s32[16]{0:T(128)} %param.16) | copy-start | bytes 196
  6.5 122.2 %all-reduce.4.cloned.1.call-start = ((), (), s32[]{:S(2)}) async-start(), calls=%async_computation.7 | async-start | bytes 786432 | tf_op jit(solution)/shard_map/psum | solution.py:80
  16.3 183.4 %all-gather.3.cloned.1.call-start = ((), (), s32[]{:S(2)}) async-start(), calls=%async_computation.5 | async-start | bytes 2228224 | tf_op jit(solution)/shard_map/all_gather | solution.py:117
  18.2 6.4 %copy-start.11 = (f32[16]{0:T(128)S(1)}, f32[16]{0:T(128)}, u32[]{:S(2)}) copy-start(f32[16]{0:T(128)} %param.22) | copy-start | bytes 196
  133.7 6.5 %copy-start.9 = (bf16[2048]{0:T(1024)(128)(2,1)S(1)}, bf16[2048]{0:T(1024)(128)(2,1)}, u32[]{:S(2)}) copy-start(bf16[2048]{0:T(1024)(128)(2,1)} %param.25) | copy-start | bytes 12292
  133.7 6.5 %copy-start.7 = (bf16[4096]{0:T(1024)(128)(2,1)S(1)}, bf16[4096]{0:T(1024)(128)(2,1)}, u32[]{:S(2)}) copy-start(bf16[4096]{0:T(1024)(128)(2,1)} %param.27) | copy-start | bytes 24580
  133.7 6.5 %copy-start.5 = (f32[16,2048]{1,0:T(8,128)S(1)}, f32[16,2048]{1,0:T(8,128)}, u32[]{:S(2)}) copy-start(f32[16,2048]{1,0:T(8,128)} %get-tuple-element.16) | copy-start | bytes 393220
  140.1 62.1 %copy-start.4 = (bf16[2048,256]{1,0:T(8,128)(2,1)S(1)}, bf16[2048,256]{1,0:T(8,128)(2,1)}, u32[]{:S(2)}) copy-start(bf16[2048,256]{1,0:T(8,128)(2,1)} %param.26) | copy-start | bytes 3145732
  140.1 62.1 %copy-start.6 = (f32[16,2048]{1,0:T(8,128)S(1)}, f32[16,2048]{1,0:T(8,128)}, u32[]{:S(2)}) copy-start(f32[16,2048]{1,0:T(8,128)} %get-tuple-element.18) | copy-start | bytes 393220
  140.1 69.7 %reduce-scatter.10.cloned.1.call-start = ((), (), s32[]{:S(2)}) async-start(), calls=%async_computation.6 | async-start | bytes 98304
  201.5 9.2 %copy-start.8 = (bf16[16,128]{1,0:T(8,128)(2,1)S(1)}, bf16[16,128]{1,0:T(8,128)(2,1)}, u32[]{:S(2)}) copy-start(bf16[16,128]{1,0:T(8,128)(2,1)} %param.15) | copy-start | bytes 12292
  203.3 128.3 %reduce-scatter.6.cloned.1.call-start = ((), (), s32[]{:S(2)}) async-start(), calls=%async_computation.3 | async-start | bytes 278528 | tf_op jit(solution)/shard_map/reduce_scatter | solution.py:153
  258.3 79.3 %reduce-scatter.8.cloned.1.call-start = ((), (), s32[]{:S(2)}) async-start(), calls=%async_computation.4 | async-start | bytes 24576 | tf_op jit(solution)/shard_map/reduce_scatter | solution.py:154
Sparse Core Ops, SparseCore 0:
  16.5 112.2 all-reduce.3
  140.2 59.4 all-gather.2
  203.5 6.3 reduce-scatter.9
  258.4 73.1 reduce-scatter.5
  333.7 3.8 reduce-scatter.7
